TPU v7x, 32 devices: a whole 2x2x4 slice. The times are simulated.
32 devices in a mesh: grp: 2 (over y), fs: 4 (over z), tp: 4 (over x, core).
Axes of the slice: x: 2, y: 2, z: 4, core: 2. Of those that a mesh axis runs over, the one named last changes fastest.
Arguments:
- tokens: bfloat16 [4096, 2048], P(('grp', 'fs')), parts along dimension 0, may hold values from -6 to 6
- pre_gain: float32 [2048], replicated, may hold values from 0.1 to 1.9
- up_weight: float32 [2048, 8192], P('fs', 'tp'), may hold values from -0.125 to 0.125
- up_scale: float32 [8192], P('tp'), may hold values from 0.3 to 3
- down_weight: float32 [8192, 2048], P('tp', 'fs'), may hold values from -0.0625 to 0.0625
- down_scale: float32 [2048], P('fs'), may hold values from 0.3 to 3
- post_gain: float32 [2048], replicated, may hold values from 0.1 to 1.9
Outputs:
- mixed: bfloat16 [4096, 2048], P(('grp', 'fs')), parts along dimension 0
There are 2 independent parts, one for each index of `grp`. A program takes and returns all parts, laid end to end along the dimension named above; an argument that names none is the same for every part. Nothing has to cross between parts.
All inputs are finite; a program needn't handle non-finite values.
Results may differ from a plain program's by a relative error of at most 0.01.
Values may be sent and summed in bfloat16 or wider, within the bound.
A program may use at most 64 MiB of HBM per device.

v0:
```python
import jax
import jax.numpy as jnp
from jax import lax
from jax.sharding import PartitionSpec as P

epsilon = 1e-06


def rms_rows(values, scaling):
    return values * lax.rsqrt(jnp.mean(values * values, axis=-1, keepdims=True) + epsilon) * scaling


def activate(lifted, up_scale):
    return jnp.square(jax.nn.relu(lifted * up_scale)).astype(jnp.bfloat16)


def on_device(tokens, pre_gain, up_weight, up_scale, down_weight, down_scale, post_gain):
    residual = tokens.astype(jnp.float32)
    normed = rms_rows(residual, pre_gain).astype(jnp.bfloat16)
    up_cast = up_weight.astype(jnp.bfloat16)
    down_cast = down_weight.astype(jnp.bfloat16)
    column_scales = lax.all_gather(down_scale, "fs", axis=0, tiled=True)
    up_full, down_full = (
        lax.all_gather(up_cast, "fs", axis=0, tiled=True),
        lax.all_gather(down_cast, "fs", axis=1, tiled=True),
    )
    lifted = jnp.dot(normed, up_full, preferred_element_type=jnp.float32)
    hidden = activate(lifted, up_scale)
    partials = jnp.dot(hidden, down_full, preferred_element_type=jnp.float32)
    partials = (partials * column_scales).astype(jnp.bfloat16)
    summed = lax.psum(partials, "tp").astype(jnp.float32)
    branch = lax.optimization_barrier(summed.astype(jnp.bfloat16)).astype(jnp.float32)
    return (residual + rms_rows(branch, post_gain)).astype(jnp.bfloat16)


def solution(mesh):
    placed = (P(("grp", "fs"), None), P(), P("fs", "tp"), P("tp"), P("tp", "fs"), P("fs"), P())
    return jax.shard_map(
        on_device, mesh=mesh, in_specs=placed, out_specs=P(("grp", "fs"), None), check_vma=False
    )
```

profile of v0, /device:TPU:1, one launch (start us, length us, event | category | flops | bytes accessed | tf_op | source)
XLA Modules:
  0.0 389.8 jit_solution(1393398002839084678)
XLA Ops:
  6.5 0.0 all-gather.4.cloned.1.call-start
  6.5 3.8 convert_element_type.28
  10.4 0.0 all-gather.4.cloned.1.call-update
  10.4 0.0 copy-start.2
  10.4 0.0 copy-start
  10.4 0.0 copy-start.3
  10.4 0.0 copy-start.4
  10.5 0.0 all-gather.6.cloned.1.call-start
  10.5 3.9 %convert_element_type.30 = bf16[2048,512]{1,0:T(8,128)(2,1)} convert(f32[2048,512]{1,0:T(8,128)} %param.11) | non-fusion elementwise | flops 1048576 | bytes 6291456 | tf_op jit(solution)/shard_map/convert_element_type | solution.py:21
  14.4 0.0 all-gather.6.cloned.1.call-update
  14.4 0.0 all-reduce.2.cloned.1.call-start
  14.5 0.0 copy-done.2
  14.5 10.4 %all-gather = f32[4,1,512]{2,1,0:T(1,128)S(1)} all-gather(f32[1,1,512]{2,1,0:T(1,128)S(1)} %bitcast.10), channel_id=1, replica_groups=mesh['grp'=2,'fs'=4,'tp'=4] {'fs'}, dimensions={0}, use_global_device_ids=true | all-gather | bytes 10240 | tf_op jit(solution)/shard_map/all_gather | solution.py:22
  24.9 0.0 copy-done
  24.9 0.5 fusion.2
  25.4 137.0 %all-gather.4.cloned.1.call-done = bf16[2048,2048]{1,0:T(8,128)(2,1)} async-done(((bf16[512,2048]{1,0:T(8,128)(2,1)}), bf16[2048,2048]{1,0:T(8,128)(2,1)}) %all-gather.4.cloned.1.call-update) | async-done | bytes 8388624 | tf_op jit(solution)/shard_map/all_gather | solution.py:24
  162.4 149.4 %all-gather.6.cloned.1.call-done = bf16[2048,2048]{1,0:T(8,128)(2,1)} async-done(((bf16[2048,512]{1,0:T(8,128)(2,1)}), bf16[2048,2048]{1,0:T(8,128)(2,1)}) %all-gather.6.cloned.1.call-update) | async-done | bytes 8388624 | tf_op jit(solution)/shard_map/all_gather | solution.py:25
  311.8 0.0 copy-done.3
  311.8 0.0 copy-done.4
  311.8 16.0 %multiply_convert_fusion = bf16[512,2048]{1,0:T(8,128)(2,1)} fusion(bf16[2048,2048]{1,0:T(8,128)(2,1)} %all-gather.6.cloned.1.call-done, f32[2048]{0:T(1024)S(1)} %bitcast.9, bf16[2048,2048]{1,0:T(8,128)(2,1)} %all-gather.4.cloned.1.call-done, bf16[512,2048]{1,0:T(8,128)(2,1)S(1)} %copy-done, f32[2048]{0:T(1024)S(1)} %copy-done.3, f32[2048]{0:T(1024)S(1)} %copy-done.4, ...), kind=kOutput, calls=%fused_computation.11 | convolution fusion | flops 8600420352 | bytes 20998144 | tf_op jit(solution)/shard_map/dot_general | solution.py:29
  327.8 0.0 copy-start.1
  327.8 0.0 all-reduce.2.cloned.1.call-update
  327.8 49.3 %all-reduce.2.cloned.1.call-done = bf16[512,2048]{1,0:T(8,128)(2,1)} async-done(((bf16[512,2048]{1,0:T(8,128)(2,1)}), bf16[512,2048]{1,0:T(8,128)(2,1)}) %all-reduce.2.cloned.1.call-update) | async-done | bytes 2097168 | tf_op jit(solution)/shard_map/psum | solution.py:31
  377.1 2.1 fusion
  379.2 0.0 copy-done.1
  379.2 4.1 %fusion.5 = bf16[512,2048]{1,0:T(8,128)(2,1)} fusion(bf16[512,2048]{1,0:T(8,128)(2,1)} %all-reduce.2.cloned.1.call-done, bf16[512,2048]{1,0:T(8,128)(2,1)S(1)} %copy-done, f32[2048]{0:T(1024)S(1)} %copy-done.1, f32[512]{0:T(512)S(1)} %add_rsqrt_fusion), kind=kLoop, calls=%fused_computation.10 | loop fusion | flops 6291456 | bytes 6301696 | tf_op jit(solution)/shard_map/convert_element_type | solution.py:33
  (2 shorter events, 0.0 us)
Async XLA Ops:
  6.5 155.9 %all-gather.4.cloned.1.call-start = ((), (), s32[]{:S(2)}) async-start(), calls=%async_computation | async-start | bytes 10485760 | tf_op jit(solution)/shard_map/all_gather | solution.py:24
  10.4 4.1 %copy-start.2 = (f32[512]{0:T(512)S(1)}, f32[512]{0:T(512)}, u32[]{:S(2)}) copy-start(f32[512]{0:T(512)} %param.12) | copy-start | bytes 6148
  10.4 14.5 %copy-start = (bf16[512,2048]{1,0:T(8,128)(2,1)S(1)}, bf16[512,2048]{1,0:T(8,128)(2,1)}, u32[]{:S(2)}) copy-start(bf16[512,2048]{1,0:T(8,128)(2,1)} %param.7) | copy-start | bytes 6291460
  10.4 301.4 %copy-start.3 = (f32[2048]{0:T(1024)S(1)}, f32[2048]{0:T(1024)}, u32[]{:S(2)}) copy-start(f32[2048]{0:T(1024)} %param.10) | copy-start | bytes 24580
  10.4 301.4 %copy-start.4 = (f32[2048]{0:T(1024)S(1)}, f32[2048]{0:T(1024)}, u32[]{:S(2)}) copy-start(f32[2048]{0:T(1024)} %param.8) | copy-start | bytes 24580
  10.5 301.4 %all-gather.6.cloned.1.call-start = ((), (), s32[]{:S(2)}) async-start(), calls=%async_computation.1 | async-start | bytes 10485760 | tf_op jit(solution)/shard_map/all_gather | solution.py:25
  14.4 362.7 %all-reduce.2.cloned.1.call-start = ((), (), s32[]{:S(2)}) async-start(), calls=%async_computation.2 | async-start | bytes 4194304 | tf_op jit(solution)/shard_map/psum | solution.py:31
  327.8 51.4 %copy-start.1 = (f32[2048]{0:T(1024)S(1)}, f32[2048]{0:T(1024)}, u32[]{:S(2)}) copy-start(f32[2048]{0:T(1024)} %param.13) | copy-start | bytes 24580
Sparse Core Ops, SparseCore 0:
  10.5 151.8 all-gather.3
  164.0 147.7 all-gather.5
  328.0 49.1 all-reduce.1
where the time goes:
time: 391 us; the launch traced here: 390 us
  waiting for transfers between devices  336 us (86%)
  matrix products  16 us (4%)
  other arithmetic  14.4 us (4%)
  between operations  13.2 us (3%)
  blocking collectives  10.4 us (3%)
    all_gather x1, waiting for transfers between devices, on_device(): lax.all_gather(down_cast, 'fs', axis=1, tiled=True)  149 us
    all_gather x1, waiting for transfers between devices, on_device(): lax.all_gather(up_cast, 'fs', axis=0, tiled=True)  137 us
    psum x1, waiting for transfers between devices, on_device(): summed = lax.psum(partials, 'tp').astype(jnp.float32)  49.3 us
    dot_general x1, matrix products, on_device(): partials = jnp.dot(hidden, down_full, preferred_element_type=jnp.float32)  16 us
    all_gather x1, blocking collectives, on_device(): column_scales = lax.all_gather(down_scale, 'fs', axis=0, tiled=True)  10.4 us
  transfers between devices with their start and end apart: 3, of which 3 were waited for; matrix products, arithmetic and copies ran while one was open for 1% of the time, Pallas kernels for 0%

commit v1 on v0

--- a/solution.py
+++ b/solution.py
@@ -1,9 +1,15 @@
+import functools
+
 import jax
 import jax.numpy as jnp
 from jax import lax
+from jax.experimental import pallas as pl
+from jax.experimental.pallas import tpu as pltpu
 from jax.sharding import PartitionSpec as P
 
 epsilon = 1e-06
+MESH = pl.DeviceIdType.MESH
+CHUNKS = 2
 
 
 def rms_rows(values, scaling):
@@ -14,7 +20,7 @@
     return jnp.square(jax.nn.relu(lifted * up_scale)).astype(jnp.bfloat16)
 
 
-def on_device(tokens, pre_gain, up_weight, up_scale, down_weight, down_scale, post_gain):
+def plain(tokens, pre_gain, up_weight, up_scale, down_weight, down_scale, post_gain):
     residual = tokens.astype(jnp.float32)
     normed = rms_rows(residual, pre_gain).astype(jnp.bfloat16)
     up_cast = up_weight.astype(jnp.bfloat16)
@@ -33,8 +39,293 @@
     return (residual + rms_rows(branch, post_gain)).astype(jnp.bfloat16)
 
 
+def kernel(nc, normed, up_in, down_in, up_scale, down_scale, out, up, down, tok, hid, scl, keep, core_out, core_in,
+           x_out, x_in, branch, ship, send, wrecv, tok_recv, scl_recv, core_recv, x_recv, br_recv, local):
+    g, z, t = lax.axis_index("grp"), lax.axis_index("fs"), lax.axis_index("tp")
+    core, x = lax.rem(t, 2), t // 2
+    pair = z // 2
+    outer, inner, other = 3 * pair, 1 + pair, 2 - pair
+    outer2 = 3 - outer
+    is_outer = z == outer
+    n_tp = 4
+    rows = normed.shape[0]
+    depth, half = up_in.shape[1], up_in.shape[2]
+    du, dc = depth // nc, down_in.shape[2]
+    quarter = rows // n_tp
+    core_peer, x_peer = x * 2 + 1 - core, (1 - x) * 2 + core
+
+    barrier = pltpu.get_barrier_semaphore()
+    peers = [{"fs": lax.rem(z + o, 4)} for o in range(1, 4)] + [{"grp": 1 - g}]
+    peers += [{"tp": lax.rem(t + o, n_tp)} for o in range(1, n_tp)]
+    for peer in peers:
+        pl.semaphore_signal(barrier, inc=1, device_id=peer, device_id_type=MESH)
+    pl.semaphore_wait(barrier, len(peers))
+
+    def remote(src, dst, s, r, peer):
+        return pltpu.make_async_remote_copy(src_ref=src, dst_ref=dst, send_sem=send.at[s], recv_sem=r,
+                                            device_id=peer, device_id_type=MESH)
+
+    def up_slot(zz, c, h):
+        return up.at[h, pl.ds(pl.multiple_of(zz * depth + c * du, du), du), :]
+
+    def down_slot(zz, c, h):
+        return down.at[zz * nc + c, pl.ds(pl.multiple_of(h * half, half), half), :]
+
+    def up_src(c, h):
+        return up_in.at[h, pl.ds(c * du, du), :]
+
+    def down_src(c, h):
+        return down_in.at[c, pl.ds(pl.multiple_of(h * half, half), half), :]
+
+    slots, sources = (up_slot, down_slot), (up_src, down_src)
+
+    def tok_slot(n, q):
+        return tok.at[pl.ds(pl.multiple_of(n * rows + q * quarter, quarter), quarter), :]
+
+    def weight(kind, src, zz, c, h, s, peer):
+        return remote(src, slots[kind](zz, c, h), s, wrecv.at[kind, zz, c, h], peer)
+
+    def arrived(kind, zz, c, h):
+        slot = slots[kind](zz, c, h)
+        weight(kind, slot, zz, c, h, 0, {"fs": z}).wait_recv()
+
+    def block(b):
+        return branch.at[b]
+
+    @pl.when(is_outer)
+    def _():
+        started = []
+        to = {"fs": inner}
+
+        def go(copy):
+            copy.start()
+            started.append(copy)
+
+        go(remote(down_scale, scl.at[z], 0, scl_recv.at[z], to))
+        go(remote(down_scale, scl.at[z], 1, scl_recv.at[z], {"fs": other}))
+        for c in range(nc):
+            go(weight(0, up_src(c, g), z, c, g, 2 + c, to))
+        mine = normed.at[pl.ds(pl.multiple_of(t * quarter, quarter), quarter), :]
+        go(remote(mine, tok_slot(1, t), 2 + nc, tok_recv.at[t], to))
+        for c in range(nc):
+            go(weight(0, up_src(c, 1 - g), z, c, 1 - g, 3 + nc + c, to))
+        for c in range(nc):
+            go(weight(1, down_src(c, g), z, c, g, 3 + 2 * nc + c, to))
+        for c in range(nc):
+            go(weight(1, down_src(c, 1 - g), z, c, 1 - g, 3 + 3 * nc + c, to))
+        for copy in started:
+            copy.wait_send()
+        for b in range(4 * nc):
+            remote(block(b), block(b), 0, br_recv.at[b], to).wait_recv()
+
+    @pl.when(jnp.logical_not(is_outer))
+    def _():
+        started = []
+        counter = [0]
+
+        def fresh():
+            counter[0] += 1
+            return counter[0] - 1
+
+        def go(copy):
+            copy.start()
+            started.append(copy)
+
+        across, beside = {"fs": other}, {"grp": 1 - g}
+        for c in range(nc):
+            go(weight(0, up_src(c, g), z, c, g, fresh(), across))
+        go(remote(down_scale, scl.at[z], fresh(), scl_recv.at[z], across))
+        locals_ = [
+            pltpu.make_async_copy(normed, tok.at[pl.ds(0, rows), :], local.at[0]),
+            pltpu.make_async_copy(down_scale, scl.at[z], local.at[1]),
+        ]
+        for h in range(2):
+            locals_.append(pltpu.make_async_copy(
+                up_in.at[h], up.at[h, pl.ds(pl.multiple_of(z * depth, depth), depth), :], local.at[2 + h]))
+        for c in range(nc):
+            locals_.append(pltpu.make_async_copy(down_in.at[c], down.at[z * nc + c], local.at[4 + c]))
+        for copy in locals_:
+            copy.start()
+
+        def forward(kind, c):
+            arrived(kind, outer, c, g)
+            go(weight(kind, slots[kind](outer, c, g), outer, c, g, fresh(), across))
+
+        def relay(kind, zz, c):
+            arrived(kind, zz, c, g)
+            go(weight(kind, slots[kind](zz, c, g), zz, c, g, fresh(), beside))
+
+        for c in range(nc):
+            forward(0, c)
+            relay(0, other, c)
+        for c in range(nc):
+            go(weight(1, down_src(c, g), z, c, g, fresh(), across))
+        remote(tok_slot(1, t), tok_slot(1, t), 0, tok_recv.at[t], {"fs": outer}).wait_recv()
+        for o in range(1, n_tp):
+            go(remote(tok_slot(1, t), tok_slot(1, t), fresh(), tok_recv.at[t], {"tp": lax.rem(t + o, n_tp)}))
+        for copy in locals_:
+            copy.wait()
+        for c in range(nc):
+            relay(0, outer2, c)
+        for o in range(1, n_tp):
+            q = lax.rem(t + o, n_tp)
+            remote(tok_slot(1, q), tok_slot(1, q), 0, tok_recv.at[q], {"tp": q}).wait_recv()
+
+        tile = dc
+
+        def lift(h):
+            def one(i, _):
+                columns = pl.ds(pl.multiple_of(i * tile, tile), tile)
+                whole = pl.ds(pl.multiple_of(h * half + i * tile, tile), tile)
+                for n in range(2):
+                    part = pl.ds(n * rows, rows)
+                    lifted = jnp.dot(tok[part, :], up[h, :, columns], preferred_element_type=jnp.float32)
+                    hid[part, whole] = activate(lifted, up_scale[:, whole])
+                return 0
+            lax.fori_loop(0, half // tile, one, 0)
+
+        lift(g)
+        relay(1, other, 0)
+        for c in range(nc):
+            arrived(0, outer, c, 1 - g)
+            arrived(0, other, c, 1 - g)
+            arrived(0, outer2, c, 1 - g)
+        lift(1 - g)
+        for c in range(1, nc):
+            relay(1, other, c)
+
+        def project(zz, c):
+            b = zz * nc + c
+            theirs = jnp.dot(hid[pl.ds(pl.multiple_of((1 - core) * rows, rows), rows), :], down[b],
+                             preferred_element_type=jnp.float32)
+            core_out[b] = theirs.astype(jnp.bfloat16)
+            go(remote(core_out.at[b], core_in.at[b], fresh(), core_recv.at[b], {"tp": core_peer}))
+            keep[lax.rem(b, 2)] = jnp.dot(hid[pl.ds(pl.multiple_of(core * rows, rows), rows), :], down[b],
+                              preferred_element_type=jnp.float32)
+
+        def cross(zz, c):
+            b = zz * nc + c
+            remote(core_out.at[b], core_in.at[b], 0, core_recv.at[b], {"tp": core_peer}).wait_recv()
+            x_out[b] = (keep[lax.rem(b, 2)] + core_in[b].astype(jnp.float32)).astype(jnp.bfloat16)
+            go(remote(x_out.at[b], x_in.at[b], fresh(), x_recv.at[b], {"tp": x_peer}))
+
+        last = []
+        for _ in range(4 * nc):
+            last.append((fresh(), fresh()))
+
+        def finish(i, zz, c):
+            b = zz * nc + c
+            remote(x_out.at[b], x_in.at[b], 0, x_recv.at[b], {"tp": x_peer}).wait_recv()
+            total = x_out[b].astype(jnp.float32) + x_in[b].astype(jnp.float32)
+            value = (total * scl[zz, :, pl.ds(c * dc, dc)]).astype(jnp.bfloat16)
+
+            @pl.when(core == 0)
+            def _():
+                branch[b] = value
+                remote(block(b), block(b), last[i][0], br_recv.at[b], {"tp": core_peer}).start()
+
+            @pl.when(core == 1)
+            def _():
+                ship[b] = value
+                for k in range(2):
+                    remote(ship.at[b], block(b), last[i][k], br_recv.at[b], {"fs": outer, "tp": x * 2 + k}).start()
+
+        for zz in (outer, other, outer2):
+            remote(down_scale, scl.at[zz], 0, scl_recv.at[zz], {"fs": zz}).wait_recv()
+
+        order = [(z, c) for c in range(nc)] + [(other, c) for c in range(nc)]
+        for c in range(nc):
+            order += [(outer2, c), (outer, c)]
+        n = len(order)
+        for i in range(n + 2):
+            if i < n:
+                zz, c = order[i]
+                if i >= nc:
+                    arrived(1, zz, c, 1 - g)
+                project_now = True
+            else:
+                project_now = False
+            if 0 <= i - 1 < n:
+                cross(*order[i - 1])
+            if project_now:
+                project(*order[i])
+            if 0 <= i - 2 < n:
+                finish(i - 2, *order[i - 2])
+            if i < nc:
+                forward(1, i)
+            elif i < 2 * nc:
+                relay(1, outer2, i - nc)
+        for copy in started:
+            copy.wait_send()
+        for i, (zz, c) in enumerate(order):
+            b = zz * nc + c
+
+            @pl.when(core == 0)
+            def _():
+                remote(block(b), block(b), last[i][0], br_recv.at[b], {"tp": core_peer}).wait_send()
+
+            @pl.when(core == 1)
+            def _():
+                for k in range(2):
+                    remote(ship.at[b], block(b), last[i][k], br_recv.at[b], {"fs": outer, "tp": x * 2 + k}).wait_send()
+                remote(block(b), block(b), last[i][0], br_recv.at[b], {"tp": core_peer}).wait_recv()
+
+    for b in range(4 * nc):
+        out[:, b * dc:(b + 1) * dc] = branch[b]
+
+
+def fused(tokens, pre_gain, up_weight, up_scale, down_weight, down_scale, post_gain):
+    nc = CHUNKS
+    rows, width = tokens.shape
+    depth, ff = up_weight.shape
+    half, dc = ff // 2, depth // nc
+    residual = tokens.astype(jnp.float32)
+    normed = rms_rows(residual, pre_gain).astype(jnp.bfloat16)
+    up_in = up_weight.astype(jnp.bfloat16).reshape(depth, 2, half).transpose(1, 0, 2)
+    down_in = down_weight.astype(jnp.bfloat16).reshape(ff, nc, dc).transpose(1, 0, 2)
+    blocks = 4 * nc
+    bf, f32 = jnp.bfloat16, jnp.float32
+    dma = pltpu.SemaphoreType.DMA
+    anywhere, vmem = pl.BlockSpec(memory_space=pl.ANY), pl.BlockSpec(memory_space=pltpu.VMEM)
+    branch = pl.pallas_call(
+        functools.partial(kernel, nc),
+        out_shape=jax.ShapeDtypeStruct((rows, width), bf),
+        in_specs=[anywhere, anywhere, anywhere, vmem, vmem],
+        out_specs=vmem,
+        scratch_shapes=[
+            pltpu.VMEM((2, width, half), bf),
+            pltpu.VMEM((blocks, ff, dc), bf),
+            pltpu.VMEM((2 * rows, width), bf),
+            pltpu.VMEM((2 * rows, ff), bf),
+            pltpu.VMEM((4, 1, depth), f32),
+            pltpu.VMEM((2, rows, dc), f32),
+            pltpu.VMEM((blocks, rows, dc), bf),
+            pltpu.VMEM((blocks, rows, dc), bf),
+            pltpu.VMEM((blocks, rows, dc), bf),
+            pltpu.VMEM((blocks, rows, dc), bf),
+            pltpu.VMEM((blocks, rows, dc), bf),
+            pltpu.VMEM((blocks, rows, dc), bf),
+            dma((64 * nc,)),
+            dma((2, 4, nc, 2)),
+            dma((4,)),
+            dma((4,)),
+            dma((blocks,)),
+            dma((blocks,)),
+            dma((blocks,)),
+            dma((4 + nc,)),
+        ],
+        compiler_params=pltpu.CompilerParams(
+            collective_id=0, has_side_effects=True, vmem_limit_bytes=60 << 20
+        ),
+    )(normed, up_in, down_in, up_scale.reshape(1, ff), down_scale.reshape(1, depth))
+    branch = branch.astype(jnp.float32)
+    return (residual + rms_rows(branch, post_gain)).astype(jnp.bfloat16)
+
+
 def solution(mesh):
     placed = (P(("grp", "fs"), None), P(), P("fs", "tp"), P("tp"), P("tp", "fs"), P("fs"), P())
+    sizes = mesh.shape
+    line = sizes["grp"] == 2 and sizes["fs"] == 4 and sizes["tp"] == 4
     return jax.shard_map(
-        on_device, mesh=mesh, in_specs=placed, out_specs=P(("grp", "fs"), None), check_vma=False
+        fused if line else plain, mesh=mesh, in_specs=placed, out_specs=P(("grp", "fs"), None), check_vma=False
     )

time: 391 us -> 168 us (0.43)
  waiting for transfers between devices: 336 us -> 0 us
  Pallas kernels: 0 us -> 145 us
  matrix products: 16 us -> 0 us
  between operations: 13.2 us -> 0.05 us
  local copies, waits for them, and re-layouts: 0.03 us -> 11.8 us
  blocking collectives: 10.4 us -> 0 us
    all_gather x2 -> x0, waiting for transfers between devices: 286 us -> none  [the longest x1 149 us: on_device(): lax.all_gather(down_cast, 'fs', axis=1, tiled=True)]
    pallas_call x0 -> x1, Pallas kernels: none -> 145 us  [fused(): pl.pallas_call(functools.partial(kernel, nc), out_shape=jax.ShapeDtypeStr...]
    psum x1 -> x0, waiting for transfers between devices: 49.3 us -> none  [on_device(): summed = lax.psum(partials, 'tp').astype(jnp.float32)]
    dot_general x1 -> x0, matrix products: 16 us -> none  [on_device(): partials = jnp.dot(hidden, down_full, preferred_element_type=jnp.float32)]
    all_gather x1 -> x0, blocking collectives: 10.4 us -> none  [on_device(): column_scales = lax.all_gather(down_scale, 'fs', axis=0, tiled=True)]
    unnamed x10 -> x6, local copies, waits for them, and re-layouts: 0.03 us -> 6.75 us
    reshape x0 -> x2, local copies, waits for them, and re-layouts: none -> 5.02 us  [the longest x1 2.53 us: fused(): up_weight.astype(jnp.bfloat16).reshape(depth, 2, half).transpose(1, 0, 2)]
    convert_element_type x3 -> x2, other arithmetic: 11.8 us -> 7.55 us  [the longest x1 4.09 us: fused(): return (residual + rms_rows(branch, post_gain)).astype(jnp.bfloat16)]
  transfers between devices with their start and end apart: 3 -> 0, of which waited for: 3 -> 0; matrix products, arithmetic and copies ran while one was open for 1% -> 0% of each run, Pallas kernels for 0% -> 0%
where the time goes in v1:
time: 168 us
  Pallas kernels  145 us (86%)
  local copies, waits for them, and re-layouts  11.8 us (7%)
  other arithmetic  11.7 us (7%)
    pallas_call x1, Pallas kernels, fused(): pl.pallas_call(functools.partial(kernel, nc), out_shape=jax.ShapeDtypeStr...  145 us
    unnamed x6, local copies, waits for them, and re-layouts  6.75 us
    reduce_sum x2, other arithmetic, rms_rows(): jnp.mean(values * values, axis=-1, keepdims=True) + epsilon  4.15 us
    convert_element_type x1, other arithmetic, fused(): return (residual + rms_rows(branch, post_gain)).astype(jnp.bfloat16)  4.09 us
    convert_element_type x1, other arithmetic, fused(): normed = rms_rows(residual, pre_gain).astype(jnp.bfloat16)  3.46 us

profile of v1, /device:TPU:1, one launch (start us, length us, event | category | flops | bytes accessed | tf_op | source)
XLA Modules:
  0.0 168.1 jit_solution(17139201407189761285)
XLA Ops:
  0.0 2.1 %fusion.2 = f32[512]{0:T(512)S(1)} fusion(bf16[512,2048]{1,0:T(8,128)(2,1)} %param.7), kind=kLoop, calls=%fused_computation.7 | loop fusion | flops 3145216 | bytes 2099200 | tf_op jit(solution)/shard_map/reduce_sum | solution.py:16
  2.1 3.5 %fusion.4.normed = bf16[512,2048]{1,0:T(8,128)(2,1)} fusion(bf16[512,2048]{1,0:T(8,128)(2,1)} %param.7, f32[2048]{0:T(1024)} %param.8, f32[512]{0:T(512)S(1)} %add_rsqrt_fusion.1), kind=kLoop, calls=%fused_computation.9 | loop fusion | flops 4194304 | bytes 4204544 | tf_op jit(solution)/shard_map/convert_element_type | solution.py:283
  5.5 3.3 %copy.8 = bf16[512,2048]{0,1:T(8,128)(2,1)S(1)} copy(f32[512,2048]{1,0:T(8,128)} %param.9) | data formatting | bytes 6291456 | tf_op args[2]
  8.9 2.5 %copy.9 = bf16[512,2,1024]{2,0,1:T(8,128)(2,1)} copy(bf16[512,2,1024]{0,2,1:T(8,128)(2,1)S(1)} %bitcast.6) | data formatting | bytes 4194304 | tf_op jit(solution)/shard_map/reshape | solution.py:284
  11.4 3.4 %copy.10 = bf16[2048,512]{0,1:T(8,128)(2,1)S(1)} copy(f32[2048,512]{1,0:T(8,128)} %param.11) | data formatting | bytes 6291456 | tf_op args[4]
  14.8 2.5 %copy.11 = bf16[2048,2,256]{2,0,1:T(8,128)(2,1)} copy(bf16[2048,2,256]{0,2,1:T(8,128)(2,1)S(1)} %bitcast.7) | data formatting | bytes 4194304 | tf_op jit(solution)/shard_map/reshape | solution.py:285
  17.3 0.0 copy-start
  17.3 0.0 copy-start.1
  17.3 144.6 %shard_map.73 = bf16[512,2048]{1,0:T(8,128)(2,1)} custom-call(bf16[512,2048]{1,0:T(8,128)(2,1)} %fusion.4.normed, bf16[2,512,1024]{2,1,0:T(8,128)(2,1)} %bitcast.8, bf16[2,2048,256]{2,1,0:T(8,128)(2,1)} %bitcast.9, f32[1,2048]{1,0:T(1,128)} %bitcast.10, f32[1,512]{1,0:T(1,128)} %bitcast.11), custom_call_target="tpu_custom_call" | custom-call | tf_op jit(solution)/shard_map/pallas_call | solution.py:290
  161.9 2.1 %fusion = f32[512]{0:T(512)S(1)} fusion(bf16[512,2048]{1,0:T(8,128)(2,1)} %shard_map.73), kind=kLoop, calls=%fused_computation.5 | loop fusion | flops 3145216 | bytes 2099200 | tf_op jit(solution)/shard_map/reduce_sum | solution.py:16
  164.0 0.0 copy-done
  164.0 0.0 copy-done.1
  164.0 4.1 %fusion.5 = bf16[512,2048]{1,0:T(8,128)(2,1)} fusion(bf16[512,2048]{1,0:T(8,128)(2,1)} %shard_map.73, bf16[512,2048]{1,0:T(8,128)(2,1)S(1)} %copy-done, f32[2048]{0:T(1024)S(1)} %copy-done.1, f32[512]{0:T(512)S(1)} %add_rsqrt_fusion), kind=kLoop, calls=%fused_computation.10 | loop fusion | flops 6291456 | bytes 6301696 | tf_op jit(solution)/shard_map/convert_element_type | solution.py:322
  (2 shorter events, 0.0 us)
Async XLA Ops:
  17.3 146.7 %copy-start = (bf16[512,2048]{1,0:T(8,128)(2,1)S(1)}, bf16[512,2048]{1,0:T(8,128)(2,1)}, u32[]{:S(2)}) copy-start(bf16[512,2048]{1,0:T(8,128)(2,1)} %param.7) | copy-start | bytes 6291460
  17.3 146.7 %copy-start.1 = (f32[2048]{0:T(1024)S(1)}, f32[2048]{0:T(1024)}, u32[]{:S(2)}) copy-start(f32[2048]{0:T(1024)} %param.13) | copy-start | bytes 24580

commit v2 on v1

--- a/solution.py
+++ b/solution.py
@@ -39,8 +39,9 @@
     return (residual + rms_rows(branch, post_gain)).astype(jnp.bfloat16)
 
 
-def kernel(nc, normed, up_in, down_in, up_scale, down_scale, out, up, down, tok, hid, scl, keep, core_out, core_in,
-           x_out, x_in, branch, ship, send, wrecv, tok_recv, scl_recv, core_recv, x_recv, br_recv, local):
+def kernel(nc, tokens, up_in, down_in, up_scale, down_scale, pre_gain, post_gain, out, res, up_f32, down_f32, up,
+           down, tok, hid, scl, keep, core_out, core_in,
+           x_out, x_in, branch, ship, send, wrecv, tok_recv, scl_recv, core_recv, x_recv, br_recv, local, one_sem):
     g, z, t = lax.axis_index("grp"), lax.axis_index("fs"), lax.axis_index("tp")
     core, x = lax.rem(t, 2), t // 2
     pair = z // 2
@@ -48,11 +49,33 @@
     outer2 = 3 - outer
     is_outer = z == outer
     n_tp = 4
-    rows = normed.shape[0]
-    depth, half = up_in.shape[1], up_in.shape[2]
-    du, dc = depth // nc, down_in.shape[2]
+    rows = tokens.shape[0]
+    depth, half = up_in.shape[0], up_in.shape[1] // 2
+    du, dc = depth // nc, depth // nc
     quarter = rows // n_tp
     core_peer, x_peer = x * 2 + 1 - core, (1 - x) * 2 + core
+
+    def at_half(h):
+        return pl.ds(pl.multiple_of(h * half, half), half)
+
+    def load(kind, c, h):
+        if kind == 0:
+            place = pl.ds(c * du, du), at_half(h)
+            pair = up_in.at[place], up_f32.at[place]
+        else:
+            place = at_half(h), pl.ds(c * dc, dc)
+            pair = down_in.at[place], down_f32.at[place]
+        return pltpu.make_async_copy(*pair, local.at[kind, c, h])
+
+    for c in range(nc):
+        load(0, c, g).start()
+    fetch = pltpu.make_async_copy(tokens, res, one_sem.at[0])
+    fetch.start()
+    for c in range(nc):
+        load(0, c, 1 - g).start()
+    for h in (g, 1 - g):
+        for c in range(nc):
+            load(1, c, h).start()
 
     barrier = pltpu.get_barrier_semaphore()
     peers = [{"fs": lax.rem(z + o, 4)} for o in range(1, 4)] + [{"grp": 1 - g}]
@@ -71,13 +94,22 @@
     def down_slot(zz, c, h):
         return down.at[zz * nc + c, pl.ds(pl.multiple_of(h * half, half), half), :]
 
-    def up_src(c, h):
-        return up_in.at[h, pl.ds(c * du, du), :]
-
-    def down_src(c, h):
-        return down_in.at[c, pl.ds(pl.multiple_of(h * half, half), half), :]
-
-    slots, sources = (up_slot, down_slot), (up_src, down_src)
+    slots = (up_slot, down_slot)
+
+    def cast(kind, c, h):
+        load(kind, c, h).wait()
+        if kind == 0:
+            up[h, pl.ds(pl.multiple_of(z * depth + c * du, du), du), :] = up_f32[
+                pl.ds(c * du, du), at_half(h)].astype(jnp.bfloat16)
+        else:
+            down[z * nc + c, at_half(h), :] = down_f32[at_half(h), pl.ds(c * dc, dc)].astype(jnp.bfloat16)
+
+    def norm_rows(first, n, step):
+        def one(i, _):
+            part = pl.ds(pl.multiple_of(first + i * step, step), step)
+            tok[part, :] = rms_rows(res[part, :].astype(jnp.float32), pre_gain[...]).astype(jnp.bfloat16)
+            return 0
+        lax.fori_loop(0, n // step, one, 0)
 
     def tok_slot(n, q):
         return tok.at[pl.ds(pl.multiple_of(n * rows + q * quarter, quarter), quarter), :]
@@ -104,15 +136,20 @@
         go(remote(down_scale, scl.at[z], 0, scl_recv.at[z], to))
         go(remote(down_scale, scl.at[z], 1, scl_recv.at[z], {"fs": other}))
         for c in range(nc):
-            go(weight(0, up_src(c, g), z, c, g, 2 + c, to))
-        mine = normed.at[pl.ds(pl.multiple_of(t * quarter, quarter), quarter), :]
-        go(remote(mine, tok_slot(1, t), 2 + nc, tok_recv.at[t], to))
-        for c in range(nc):
-            go(weight(0, up_src(c, 1 - g), z, c, 1 - g, 3 + nc + c, to))
-        for c in range(nc):
-            go(weight(1, down_src(c, g), z, c, g, 3 + 2 * nc + c, to))
-        for c in range(nc):
-            go(weight(1, down_src(c, 1 - g), z, c, 1 - g, 3 + 3 * nc + c, to))
+            cast(0, c, g)
+            go(weight(0, up_slot(z, c, g), z, c, g, 2 + c, to))
+        fetch.wait()
+        norm_rows(t * quarter, quarter, min(quarter, 64))
+        go(remote(tok_slot(0, t), tok_slot(1, t), 2 + nc, tok_recv.at[t], to))
+        for c in range(nc):
+            cast(0, c, 1 - g)
+            go(weight(0, up_slot(z, c, 1 - g), z, c, 1 - g, 3 + nc + c, to))
+        for c in range(nc):
+            cast(1, c, g)
+            go(weight(1, down_slot(z, c, g), z, c, g, 3 + 2 * nc + c, to))
+        for c in range(nc):
+            cast(1, c, 1 - g)
+            go(weight(1, down_slot(z, c, 1 - g), z, c, 1 - g, 3 + 3 * nc + c, to))
         for copy in started:
             copy.wait_send()
         for b in range(4 * nc):
@@ -133,19 +170,16 @@
 
         across, beside = {"fs": other}, {"grp": 1 - g}
         for c in range(nc):
-            go(weight(0, up_src(c, g), z, c, g, fresh(), across))
+            cast(0, c, g)
+            go(weight(0, up_slot(z, c, g), z, c, g, fresh(), across))
         go(remote(down_scale, scl.at[z], fresh(), scl_recv.at[z], across))
-        locals_ = [
-            pltpu.make_async_copy(normed, tok.at[pl.ds(0, rows), :], local.at[0]),
-            pltpu.make_async_copy(down_scale, scl.at[z], local.at[1]),
-        ]
-        for h in range(2):
-            locals_.append(pltpu.make_async_copy(
-                up_in.at[h], up.at[h, pl.ds(pl.multiple_of(z * depth, depth), depth), :], local.at[2 + h]))
-        for c in range(nc):
-            locals_.append(pltpu.make_async_copy(down_in.at[c], down.at[z * nc + c], local.at[4 + c]))
-        for copy in locals_:
-            copy.start()
+        own_scale = pltpu.make_async_copy(down_scale, scl.at[z], one_sem.at[1])
+        own_scale.start()
+        for c in range(nc):
+            cast(1, c, g)
+        fetch.wait()
+        norm_rows(0, rows, 64)
+        own_scale.wait()
 
         def forward(kind, c):
             arrived(kind, outer, c, g)
@@ -159,12 +193,14 @@
             forward(0, c)
             relay(0, other, c)
         for c in range(nc):
-            go(weight(1, down_src(c, g), z, c, g, fresh(), across))
+            go(weight(1, down_slot(z, c, g), z, c, g, fresh(), across))
         remote(tok_slot(1, t), tok_slot(1, t), 0, tok_recv.at[t], {"fs": outer}).wait_recv()
         for o in range(1, n_tp):
             go(remote(tok_slot(1, t), tok_slot(1, t), fresh(), tok_recv.at[t], {"tp": lax.rem(t + o, n_tp)}))
-        for copy in locals_:
-            copy.wait()
+        for c in range(nc):
+            cast(0, c, 1 - g)
+        for c in range(nc):
+            cast(1, c, 1 - g)
         for c in range(nc):
             relay(0, outer2, c)
         for o in range(1, n_tp):
@@ -270,8 +306,13 @@
                     remote(ship.at[b], block(b), last[i][k], br_recv.at[b], {"fs": outer, "tp": x * 2 + k}).wait_send()
                 remote(block(b), block(b), last[i][0], br_recv.at[b], {"tp": core_peer}).wait_recv()
 
-    for b in range(4 * nc):
-        out[:, b * dc:(b + 1) * dc] = branch[b]
+    def close(i, _):
+        part = pl.ds(pl.multiple_of(i * 64, 64), 64)
+        row = jnp.concatenate([branch[b, part, :] for b in range(4 * nc)], axis=1).astype(jnp.float32)
+        out[part, :] = (res[part, :].astype(jnp.float32) + rms_rows(row, post_gain[...])).astype(jnp.bfloat16)
+        return 0
+
+    lax.fori_loop(0, rows // 64, close, 0)
 
 
 def fused(tokens, pre_gain, up_weight, up_scale, down_weight, down_scale, post_gain):
@@ -279,20 +320,19 @@
     rows, width = tokens.shape
     depth, ff = up_weight.shape
     half, dc = ff // 2, depth // nc
-    residual = tokens.astype(jnp.float32)
-    normed = rms_rows(residual, pre_gain).astype(jnp.bfloat16)
-    up_in = up_weight.astype(jnp.bfloat16).reshape(depth, 2, half).transpose(1, 0, 2)
-    down_in = down_weight.astype(jnp.bfloat16).reshape(ff, nc, dc).transpose(1, 0, 2)
     blocks = 4 * nc
     bf, f32 = jnp.bfloat16, jnp.float32
     dma = pltpu.SemaphoreType.DMA
     anywhere, vmem = pl.BlockSpec(memory_space=pl.ANY), pl.BlockSpec(memory_space=pltpu.VMEM)
-    branch = pl.pallas_call(
+    return pl.pallas_call(
         functools.partial(kernel, nc),
         out_shape=jax.ShapeDtypeStruct((rows, width), bf),
-        in_specs=[anywhere, anywhere, anywhere, vmem, vmem],
+        in_specs=[anywhere, anywhere, anywhere, vmem, vmem, vmem, vmem],
         out_specs=vmem,
         scratch_shapes=[
+            pltpu.VMEM((rows, width), bf),
+            pltpu.VMEM((depth, ff), f32),
+            pltpu.VMEM((ff, depth), f32),
             pltpu.VMEM((2, width, half), bf),
             pltpu.VMEM((blocks, ff, dc), bf),
             pltpu.VMEM((2 * rows, width), bf),
@@ -312,14 +352,14 @@
             dma((blocks,)),
             dma((blocks,)),
             dma((blocks,)),
-            dma((4 + nc,)),
+            dma((2, nc, 2)),
+            dma((2,)),
         ],
         compiler_params=pltpu.CompilerParams(
             collective_id=0, has_side_effects=True, vmem_limit_bytes=60 << 20
         ),
-    )(normed, up_in, down_in, up_scale.reshape(1, ff), down_scale.reshape(1, depth))
-    branch = branch.astype(jnp.float32)
-    return (residual + rms_rows(branch, post_gain)).astype(jnp.bfloat16)
+    )(tokens, up_weight, down_weight, up_scale.reshape(1, ff), down_scale.reshape(1, depth),
+      pre_gain.reshape(1, width), post_gain.reshape(1, width))
 
 
 def solution(mesh):

time: 168 us -> 150 us (0.89)
  other arithmetic: 11.7 us -> 0 us
  local copies, waits for them, and re-layouts: 11.8 us -> 3.16 us
  Pallas kernels: 145 us -> 147 us
    convert_element_type x2 -> x0, other arithmetic: 7.55 us -> none  [the longest x1 4.09 us: fused(): return (residual + rms_rows(branch, post_gain)).astype(jnp.bfloat16)]
    reshape x2 -> x0, local copies, waits for them, and re-layouts: 5.02 us -> none  [the longest x1 2.53 us: fused(): up_weight.astype(jnp.bfloat16).reshape(depth, 2, half).transpose(1, 0, 2)]
    reduce_sum x2 -> x0, other arithmetic: 4.15 us -> none  [rms_rows(): jnp.mean(values * values, axis=-1, keepdims=True) + epsilon]
    unnamed x6 -> x1, local copies, waits for them, and re-layouts: 6.75 us -> 3.16 us
    pallas_call x1, Pallas kernels: 145 us -> 147 us  [fused(): pl.pallas_call(functools.partial(kernel, nc), out_shape=jax.ShapeDtypeStr...]
where the time goes in v2:
time: 150 us
  Pallas kernels  147 us (98%)
  local copies, waits for them, and re-layouts  3.16 us (2%)
    pallas_call x1, Pallas kernels, fused(): pl.pallas_call(functools.partial(kernel, nc), out_shape=jax.ShapeDtypeStr...  147 us
    unnamed x1, local copies, waits for them, and re-layouts  3.16 us

profile of v2, /device:TPU:1, one launch (start us, length us, event | category | flops | bytes accessed | tf_op | source)
XLA Modules:
  0.0 149.9 jit_solution(11522018145990187460)
XLA Ops:
  0.0 146.8 %shard_map.73 = bf16[512,2048]{1,0:T(8,128)(2,1)} custom-call(bf16[512,2048]{1,0:T(8,128)(2,1)} %tokens.1, f32[512,2048]{1,0:T(8,128)} %up_in.1, f32[2048,512]{1,0:T(8,128)} %down_in.1, f32[1,2048]{1,0:T(1,128)} %bitcast.4, f32[1,512]{1,0:T(1,128)} %bitcast.7, f32[1,2048]{1,0:T(1,128)} %bitcast.5, f32[1,2048]{1,0:T(1,128)} %bitcast.6), custom_call_target="tpu_custom_call" | custom-call | tf_op jit(solution)/shard_map/pallas_call | solution.py:327
  146.8 3.2 %copy.9 = bf16[512,2048]{1,0:T(8,128)(2,1)} copy(bf16[512,2048]{1,0:T(8,128)(2,1)} %shard_map.73) | data formatting | bytes 4194304
